TPU v7x, 32 devices: a whole 2x2x4 slice. The times are simulated.
32 devices in a mesh: sp: 4 (over y, core), dp: 8 (over z, x).
Axes of the slice: x: 2, y: 2, z: 4, core: 2. Of those that a mesh axis runs over, the one named last changes fastest.
Arguments:
- query_rows: bfloat16 [8, 512, 4, 128], P('dp', 'sp'), may hold values from -6 to 6
- key_rows: bfloat16 [8, 512, 4, 128], P('dp', 'sp'), may hold values from -6 to 6
- value_rows: bfloat16 [8, 512, 4, 128], P('dp', 'sp'), may hold values from -6 to 6
- map_weight: float32 [4], P('sp'), may hold values from 0.3 to 0.8
- head_gain: float32 [128], replicated, may hold values from 0.1 to 1.9
Outputs:
- mixed: bfloat16 [8, 512, 4, 128], P('dp', 'sp')
All inputs are finite; a program needn't handle non-finite values.
Results may differ from a plain program's by a relative error of at most 0.0049.
Values may be sent and summed in bfloat16 or wider, within the bound.
A program may use at most 64 MiB of HBM per device.

v0:
```python
import math
import jax
import jax.numpy as jnp
from jax import lax
from jax.sharding import PartitionSpec as P

QK = 64
SEGMENT = 64


def map_output(query_map, key_map, value_head):
    length = key_map.shape[0]
    block_len = math.gcd(length, 512)
    key_segment = jnp.arange(length, dtype=jnp.int32) // SEGMENT

    def one_block(start):
        query_block = lax.dynamic_slice_in_dim(query_map, start, block_len, 0)
        query_segment = (start + jnp.arange(block_len, dtype=jnp.int32)) // SEGMENT
        visible = key_segment[None, :] <= query_segment[:, None]
        scores = jnp.dot(query_block, key_map.T, preferred_element_type=jnp.float32) * QK ** (-0.5)
        scores = jnp.where(visible, scores, -jnp.inf)
        scores = scores - jnp.max(scores, axis=-1, keepdims=True)
        raised = jnp.exp(scores)
        weights = raised / jnp.sum(raised, axis=-1, keepdims=True)
        return jnp.dot(weights.astype(jnp.bfloat16), value_head, preferred_element_type=jnp.float32)

    starts = jnp.arange(length // block_len, dtype=jnp.int32) * block_len
    return lax.map(one_block, starts).reshape(length, value_head.shape[1])


def per_heads(query_local, key_local, value_local):
    return lax.map(
        lambda group: map_output(group[0], group[1], group[2]),
        (
            query_local[0].transpose(1, 0, 2),
            key_local[0].transpose(1, 0, 2),
            value_local[0].transpose(1, 0, 2),
        ),
    )


def finish(first_part, second_part, map_weight, head_gain):
    attended = first_part - map_weight[:, None, None] * second_part
    mean_square = jnp.mean(attended * attended, axis=-1, keepdims=True)
    normed = (attended * lax.rsqrt(mean_square + 1e-06) * head_gain).astype(jnp.bfloat16)
    return normed.transpose(1, 0, 2)[None]


def on_device(query_rows, key_rows, value_rows, map_weight, head_gain):
    query_local, key_local, value_local = (
        lax.all_to_all(query_rows, "sp", split_axis=2, concat_axis=1, tiled=True),
        lax.all_to_all(key_rows, "sp", split_axis=2, concat_axis=1, tiled=True),
        lax.all_to_all(value_rows, "sp", split_axis=2, concat_axis=1, tiled=True),
    )
    first_part = per_heads(query_local[..., :QK], key_local[..., :QK], value_local)
    second_part = per_heads(query_local[..., QK:], key_local[..., QK:], value_local)
    normed = finish(first_part, second_part, map_weight, head_gain)
    return lax.all_to_all(normed, "sp", split_axis=1, concat_axis=2, tiled=True)


def solution(mesh):
    return jax.shard_map(
        on_device,
        mesh=mesh,
        in_specs=(
            P("dp", "sp", None, None),
            P("dp", "sp", None, None),
            P("dp", "sp", None, None),
            P("sp"),
            P(),
        ),
        out_specs=P("dp", "sp", None, None),
        check_vma=False,
    )
```

profile of v0, /device:TPU:0, one launch (start us, length us, event | category | flops | bytes accessed | tf_op | source)
XLA Modules:
  0.0 37.9 jit_solution(136135858623358631)
XLA Ops:
  0.0 1.6 %copy.24 = bf16[1,128,4,128]{3,1,0,2:T(8,128)(2,1)} copy(bf16[1,128,4,128]{3,2,1,0:T(4,128)(2,1)} %param.5) | data formatting | bytes 262144 | tf_op args[0]
  1.6 0.0 copy-start
  1.6 4.4 %all-to-all-start = ((bf16[1,128,4,128]{3,1,0,2:T(8,128)(2,1)}), bf16[1,128,4,128]{3,1,0,2:T(8,128)(2,1)S(1)}, u32[]{:S(2)}, u32[]{:S(2)}) async-start(bf16[1,128,4,128]{3,1,0,2:T(8,128)(2,1)} %copy.24), calls=%async_computation | async-start | bytes 262144 | tf_op jit(solution)/shard_map/all_to_all | solution.py:51
  6.0 0.0 copy-done
  6.0 0.0 copy-start.1
  6.0 0.7 %copy.26 = bf16[1,128,4,128]{3,1,0,2:T(8,128)(2,1)} copy(bf16[1,128,4,128]{3,2,1,0:T(4,128)(2,1)S(1)} %copy-done) | data formatting | bytes 262144 | tf_op args[1]
  6.6 0.3 copy-done.1
  6.9 0.7 %copy.28 = bf16[1,128,4,128]{3,1,0,2:T(8,128)(2,1)} copy(bf16[1,128,4,128]{3,2,1,0:T(4,128)(2,1)S(1)} %copy-done.1) | data formatting | bytes 262144 | tf_op args[2]
  8.3 2.3 %all-to-all-done = bf16[1,128,4,128]{3,1,0,2:T(8,128)(2,1)S(1)} async-done(((bf16[1,128,4,128]{3,1,0,2:T(8,128)(2,1)}), bf16[1,128,4,128]{3,1,0,2:T(8,128)(2,1)S(1)}, u32[]{:S(2)}, u32[]{:S(2)}) %all-to-all-start) | async-done | bytes 131104 | tf_op jit(solution)/shard_map/all_to_all | solution.py:51
  10.6 3.3 %all-to-all-start.1 = ((bf16[1,128,4,128]{3,1,0,2:T(8,128)(2,1)}), bf16[1,128,4,128]{3,1,0,2:T(8,128)(2,1)S(1)}, u32[]{:S(2)}, u32[]{:S(2)}) async-start(bf16[1,128,4,128]{3,1,0,2:T(8,128)(2,1)} %copy.26), calls=%async_computation.1 | async-start | bytes 262144 | tf_op jit(solution)/shard_map/all_to_all | solution.py:52
  13.9 4.6 %all-to-all-done.1 = bf16[1,128,4,128]{3,1,0,2:T(8,128)(2,1)S(1)} async-done(((bf16[1,128,4,128]{3,1,0,2:T(8,128)(2,1)}), bf16[1,128,4,128]{3,1,0,2:T(8,128)(2,1)S(1)}, u32[]{:S(2)}, u32[]{:S(2)}) %all-to-all-start.1) | async-done | bytes 131104 | tf_op jit(solution)/shard_map/all_to_all | solution.py:52
  18.5 3.3 %all-to-all-start.2 = ((bf16[1,128,4,128]{3,1,0,2:T(8,128)(2,1)}), bf16[1,128,4,128]{3,1,0,2:T(8,128)(2,1)S(1)}, u32[]{:S(2)}, u32[]{:S(2)}) async-start(bf16[1,128,4,128]{3,1,0,2:T(8,128)(2,1)} %copy.28), calls=%async_computation.2 | async-start | bytes 262144 | tf_op jit(solution)/shard_map/all_to_all | solution.py:53
  21.8 0.4 %fusion.8 = (f32[512]{0:T(512)S(1)}, f32[512,512]{0,1:T(8,128)S(1)}) fusion(bf16[1,512,1,128]{3,1,2,0:T(8,128)(2,1)S(1)} %bitcast.59, bf16[1,512,1,128]{3,1,2,0:T(8,128)(2,1)S(1)} %bitcast.55, s32[512]{0:T(512)S(1)} %add_select_fusion), kind=kOutput, calls=%fused_computation.27 | convolution fusion | flops 34602496 | bytes 1316864 | tf_op jit(solution)/shard_map/while/body/eval_jaxpr/while/body/eval_jaxpr/dot_general | solution.py:20
  22.2 0.3 fusion.9
  22.5 0.2 fusion.3
  22.7 0.2 fusion.2
  22.9 3.5 %all-to-all-done.2 = bf16[1,128,4,128]{3,1,0,2:T(8,128)(2,1)S(1)} async-done(((bf16[1,128,4,128]{3,1,0,2:T(8,128)(2,1)}), bf16[1,128,4,128]{3,1,0,2:T(8,128)(2,1)S(1)}, u32[]{:S(2)}, u32[]{:S(2)}) %all-to-all-start.2) | async-done | bytes 131104 | tf_op jit(solution)/shard_map/all_to_all | solution.py:53
  26.4 0.3 convolution_multiply_fusion.2
  26.7 0.4 multiply_reduce_fusion
  27.1 0.0 copy-start.2
  27.1 0.6 %copy-done.2 = f32[128]{0:T(128)S(1)} copy-done((f32[128]{0:T(128)S(1)}, f32[128]{0:T(128)}, u32[]{:S(2)}) %copy-start.2) | copy-done | bytes 536
  27.8 0.1 fusion.4
  27.8 0.2 copy.31
  28.0 0.5 %broadcast.100 = bf16[]{:T(256)} broadcast(bf16[]{:T(256)} %constant.139), dimensions={} | broadcast | bytes 4
  28.5 1.4 %reduce.2 = bf16[512,128]{1,0:T(8,128)(2,1)S(1)} reduce(bf16[512,1,1,128]{3,2,1,0:T(2,128)(2,1)S(1)} %bitcast.52, bf16[]{:T(256)} %broadcast.100), dimensions={1,2}, to_apply=%bitcast.39.reduce_sub_computation | reduce | bytes 262146
  30.0 7.0 %all_to_all.69 = bf16[4,2,8192]{2,1,0:T(2,128)(2,1)S(1)} all-to-all(bf16[4,2,8192]{2,1,0:T(2,128)(2,1)S(1)} %reshape.64), channel_id=1, replica_groups=mesh['sp'=4,'dp'=8] {'sp'}, dimensions={0} | all-to-all | bytes 262144 | tf_op jit(solution)/shard_map/all_to_all | solution.py:58
  37.0 0.1 reshape.65
  37.1 0.8 %copy.32 = bf16[1,128,4,128]{3,2,1,0:T(4,128)(2,1)} copy(bf16[1,128,4,128]{3,1,2,0:T(8,128)(2,1)S(1)} %bitcast.54) | data formatting | bytes 262144 | tf_op jit(solution)/shard_map/all_to_all | solution.py:58
  (4 shorter events, 0.1 us)
Async XLA Ops:
  1.6 4.4 %copy-start = (bf16[1,128,4,128]{3,2,1,0:T(4,128)(2,1)S(1)}, bf16[1,128,4,128]{3,2,1,0:T(4,128)(2,1)}, u32[]{:S(2)}) copy-start(bf16[1,128,4,128]{3,2,1,0:T(4,128)(2,1)} %param.6) | copy-start | bytes 393220
  1.6 9.0 %all-to-all-start = ((bf16[1,128,4,128]{3,1,0,2:T(8,128)(2,1)}), bf16[1,128,4,128]{3,1,0,2:T(8,128)(2,1)S(1)}, u32[]{:S(2)}, u32[]{:S(2)}) async-start(bf16[1,128,4,128]{3,1,0,2:T(8,128)(2,1)} %copy.24), calls=%async_computation | async-start | bytes 262144 | tf_op jit(solution)/shard_map/all_to_all | solution.py:51
  6.0 1.0 %copy-start.1 = (bf16[1,128,4,128]{3,2,1,0:T(4,128)(2,1)S(1)}, bf16[1,128,4,128]{3,2,1,0:T(4,128)(2,1)}, u32[]{:S(2)}) copy-start(bf16[1,128,4,128]{3,2,1,0:T(4,128)(2,1)} %param.7) | copy-start | bytes 393220
  10.6 7.9 %all-to-all-start.1 = ((bf16[1,128,4,128]{3,1,0,2:T(8,128)(2,1)}), bf16[1,128,4,128]{3,1,0,2:T(8,128)(2,1)S(1)}, u32[]{:S(2)}, u32[]{:S(2)}) async-start(bf16[1,128,4,128]{3,1,0,2:T(8,128)(2,1)} %copy.26), calls=%async_computation.1 | async-start | bytes 262144 | tf_op jit(solution)/shard_map/all_to_all | solution.py:52
  18.5 7.9 %all-to-all-start.2 = ((bf16[1,128,4,128]{3,1,0,2:T(8,128)(2,1)}), bf16[1,128,4,128]{3,1,0,2:T(8,128)(2,1)S(1)}, u32[]{:S(2)}, u32[]{:S(2)}) async-start(bf16[1,128,4,128]{3,1,0,2:T(8,128)(2,1)} %copy.28), calls=%async_computation.2 | async-start | bytes 262144 | tf_op jit(solution)/shard_map/all_to_all | solution.py:53
  27.1 0.7 %copy-start.2 = (f32[128]{0:T(128)S(1)}, f32[128]{0:T(128)}, u32[]{:S(2)}) copy-start(f32[128]{0:T(128)} %param.9) | copy-start | bytes 1540
where the time goes:
time: 38.4 us; the launch traced here: 37.9 us
  starting transfers between devices  11 us (29%)
  waiting for transfers between devices  10.3 us (27%)
  blocking collectives  6.99 us (18%)
  local copies, waits for them, and re-layouts  5.47 us (14%)
  other arithmetic  1.89 us (5%)
  matrix products  1.41 us (4%)
  between operations  0.75 us (2%)
    all_to_all x1, blocking collectives, on_device(): return lax.all_to_all(normed, 'sp', split_axis=1, concat_axis=2, tiled=True)  6.99 us
    all_to_all x1, waiting for transfers between devices, on_device(): lax.all_to_all(key_rows, 'sp', split_axis=2, concat_axis=1, tiled=True)  4.56 us
    unnamed x13, local copies, waits for them, and re-layouts  4.55 us
    all_to_all x1, starting transfers between devices, on_device(): lax.all_to_all(query_rows, 'sp', split_axis=2, concat_axis=1, tiled=True)  4.4 us
    all_to_all x1, waiting for transfers between devices, on_device(): lax.all_to_all(value_rows, 'sp', split_axis=2, concat_axis=1, tiled=True)  3.45 us
    all_to_all x1, starting transfers between devices, on_device(): lax.all_to_all(value_rows, 'sp', split_axis=2, concat_axis=1, tiled=True)  3.33 us
    all_to_all x1, starting transfers between devices, on_device(): lax.all_to_all(key_rows, 'sp', split_axis=2, concat_axis=1, tiled=True)  3.32 us
    all_to_all x1, waiting for transfers between devices, on_device(): lax.all_to_all(query_rows, 'sp', split_axis=2, concat_axis=1, tiled=True)  2.32 us
  transfers between devices with their start and end apart: 3, of which 3 were waited for; matrix products, arithmetic and copies ran while one was open for 6% of the time, Pallas kernels for 0%

commit v1 on v0

--- a/solution.py
+++ b/solution.py
@@ -50,7 +50,12 @@
     query_local, key_local, value_local = (
         lax.all_to_all(query_rows, "sp", split_axis=2, concat_axis=1, tiled=True),
         lax.all_to_all(key_rows, "sp", split_axis=2, concat_axis=1, tiled=True),
-        lax.all_to_all(value_rows, "sp", split_axis=2, concat_axis=1, tiled=True),
+        jnp.concatenate(
+            lax.all_to_all(
+                jnp.stack(jnp.split(value_rows, lax.axis_size("sp"), axis=2)), "sp", 0, 0
+            ),
+            axis=1,
+        ),
     )
     first_part = per_heads(query_local[..., :QK], key_local[..., :QK], value_local)
     second_part = per_heads(query_local[..., QK:], key_local[..., QK:], value_local)

time: 38.4 us -> 38.4 us (level)
  other arithmetic: 1.89 us -> 2.57 us
  waiting for transfers between devices: 10.3 us -> 9.68 us
    another operation x0 -> x1, other arithmetic: none -> 0.68 us  [on_device(): jnp.stack(jnp.split(value_rows, lax.axis_size('sp'), axis=2))]
    all_to_all x1, waiting for transfers between devices: 2.32 us -> 1.67 us  [on_device(): lax.all_to_all(query_rows, 'sp', split_axis=2, concat_axis=1, tiled=True)]
    unnamed x13 -> x12, local copies, waits for them, and re-layouts: 4.55 us -> 4.29 us
  transfers between devices with their start and end apart: 3 -> 3, of which waited for: 3 -> 3; matrix products, arithmetic and copies ran while one was open for 6% -> 7% of each run, Pallas kernels for 0% -> 0%
where the time goes in v1:
time: 38.4 us; the launch traced here: 37.9 us
  starting transfers between devices  11 us (29%)
  waiting for transfers between devices  9.68 us (25%)
  blocking collectives  6.99 us (18%)
  local copies, waits for them, and re-layouts  5.42 us (14%)
  other arithmetic  2.57 us (7%)
  matrix products  1.41 us (4%)
  between operations  0.77 us (2%)
    all_to_all x1, blocking collectives, on_device(): return lax.all_to_all(normed, 'sp', split_axis=1, concat_axis=2, tiled=True)  6.99 us
    all_to_all x1, waiting for transfers between devices, on_device(): lax.all_to_all(key_rows, 'sp', split_axis=2, concat_axis=1, tiled=True)  4.56 us
    all_to_all x1, starting transfers between devices, on_device(): lax.all_to_all(query_rows, 'sp', split_axis=2, concat_axis=1, tiled=True)  4.4 us
    unnamed x12, local copies, waits for them, and re-layouts  4.29 us
    all_to_all x1, waiting for transfers between devices, on_device(): lax.all_to_all(jnp.stack(jnp.split(value_rows, lax.axis_size('sp'), axis=...  3.45 us
    all_to_all x1, starting transfers between devices, on_device(): lax.all_to_all(jnp.stack(jnp.split(value_rows, lax.axis_size('sp'), axis=...  3.33 us
    all_to_all x1, starting transfers between devices, on_device(): lax.all_to_all(key_rows, 'sp', split_axis=2, concat_axis=1, tiled=True)  3.32 us
    all_to_all x1, waiting for transfers between devices, on_device(): lax.all_to_all(query_rows, 'sp', split_axis=2, concat_axis=1, tiled=True)  1.67 us
  transfers between devices with their start and end apart: 3, of which 3 were waited for; matrix products, arithmetic and copies ran while one was open for 7% of the time, Pallas kernels for 0%

profile of v1, /device:TPU:0, one launch (start us, length us, event | category | flops | bytes accessed | tf_op | source)
XLA Modules:
  0.0 37.9 jit_solution(7622704867988350492)
XLA Ops:
  0.0 1.6 %copy.33 = bf16[1,128,4,128]{3,1,0,2:T(8,128)(2,1)} copy(bf16[1,128,4,128]{3,2,1,0:T(4,128)(2,1)} %param.5) | data formatting | bytes 262144 | tf_op args[0]
  1.6 0.0 copy-start
  1.6 4.4 %all-to-all-start = ((bf16[1,128,4,128]{3,1,0,2:T(8,128)(2,1)}), bf16[1,128,4,128]{3,1,0,2:T(8,128)(2,1)S(1)}, u32[]{:S(2)}, u32[]{:S(2)}) async-start(bf16[1,128,4,128]{3,1,0,2:T(8,128)(2,1)} %copy.33), calls=%async_computation | async-start | bytes 262144 | tf_op jit(solution)/shard_map/all_to_all | solution.py:51
  6.0 0.0 copy-done
  6.0 0.0 copy-start.1
  6.0 0.2 fusion.8
  6.2 0.7 %copy-done.1 = bf16[1,128,4,128]{3,2,1,0:T(4,128)(2,1)S(1)} copy-done((bf16[1,128,4,128]{3,2,1,0:T(4,128)(2,1)S(1)}, bf16[1,128,4,128]{3,2,1,0:T(4,128)(2,1)}, u32[]{:S(2)}) %copy-start.1) | copy-done | bytes 131096
  6.9 0.7 %copy.35 = bf16[1,128,4,128]{3,1,0,2:T(8,128)(2,1)} copy(bf16[1,128,4,128]{3,2,1,0:T(4,128)(2,1)S(1)} %copy-done.1) | data formatting | bytes 262144 | tf_op args[1]
  8.2 0.7 %pad_maximum_fusion = bf16[4,1,128,1,128]{4,2,3,1,0:T(8,128)(2,1)} fusion(bf16[1,1,128,1,128]{4,2,3,1,0:T(8,128)(2,1)S(1)} %get-tuple-element.93, bf16[1,1,128,1,128]{4,2,3,1,0:T(8,128)(2,1)S(1)} %get-tuple-element.94, bf16[1,1,128,1,128]{4,2,3,1,0:T(8,128)(2,1)S(1)} %get-tuple-element.95, bf16[1,1,128,1,128]{4,2,3,1,0:T(8,128)(2,1)S(1)} %get-tuple-element.96), kind=kLoop, calls=%fused_computation.19 | loop fusion | flops 196608 | bytes 262144 | tf_op jit(solution)/shard_map/stack | solution.py:55
  8.9 1.7 %all-to-all-done = bf16[1,128,4,128]{3,1,0,2:T(8,128)(2,1)S(1)} async-done(((bf16[1,128,4,128]{3,1,0,2:T(8,128)(2,1)}), bf16[1,128,4,128]{3,1,0,2:T(8,128)(2,1)S(1)}, u32[]{:S(2)}, u32[]{:S(2)}) %all-to-all-start) | async-done | bytes 131104 | tf_op jit(solution)/shard_map/all_to_all | solution.py:51
  10.6 3.3 %all-to-all-start.1 = ((bf16[1,128,4,128]{3,1,0,2:T(8,128)(2,1)}), bf16[1,128,4,128]{3,1,0,2:T(8,128)(2,1)S(1)}, u32[]{:S(2)}, u32[]{:S(2)}) async-start(bf16[1,128,4,128]{3,1,0,2:T(8,128)(2,1)} %copy.35), calls=%async_computation.1 | async-start | bytes 262144 | tf_op jit(solution)/shard_map/all_to_all | solution.py:52
  13.9 4.6 %all-to-all-done.1 = bf16[1,128,4,128]{3,1,0,2:T(8,128)(2,1)S(1)} async-done(((bf16[1,128,4,128]{3,1,0,2:T(8,128)(2,1)}), bf16[1,128,4,128]{3,1,0,2:T(8,128)(2,1)S(1)}, u32[]{:S(2)}, u32[]{:S(2)}) %all-to-all-start.1) | async-done | bytes 131104 | tf_op jit(solution)/shard_map/all_to_all | solution.py:52
  18.5 3.3 %all-to-all-start.2 = ((bf16[4,1,128,1,128]{4,2,3,1,0:T(8,128)(2,1)}), bf16[4,1,128,1,128]{4,2,3,1,0:T(8,128)(2,1)S(1)}, u32[]{:S(2)}, u32[]{:S(2)}) async-start(bf16[4,1,128,1,128]{4,2,3,1,0:T(8,128)(2,1)} %pad_maximum_fusion), calls=%async_computation.2 | async-start | bytes 262144 | tf_op jit(solution)/shard_map/all_to_all | solution.py:54
  21.8 0.4 %fusion.9 = (f32[512]{0:T(512)S(1)}, f32[512,512]{0,1:T(8,128)S(1)}) fusion(bf16[1,512,1,128]{3,1,2,0:T(8,128)(2,1)S(1)} %bitcast.63, bf16[1,512,1,128]{3,1,2,0:T(8,128)(2,1)S(1)} %bitcast.59, s32[512]{0:T(512)S(1)} %add_select_fusion), kind=kOutput, calls=%fused_computation.33 | convolution fusion | flops 34602496 | bytes 1316864 | tf_op jit(solution)/shard_map/while/body/eval_jaxpr/while/body/eval_jaxpr/dot_general | solution.py:20
  22.2 0.3 fusion.10
  22.5 0.2 fusion.3
  22.7 0.2 fusion.2
  22.9 3.5 %all-to-all-done.2 = bf16[4,1,128,1,128]{4,2,3,1,0:T(8,128)(2,1)S(1)} async-done(((bf16[4,1,128,1,128]{4,2,3,1,0:T(8,128)(2,1)}), bf16[4,1,128,1,128]{4,2,3,1,0:T(8,128)(2,1)S(1)}, u32[]{:S(2)}, u32[]{:S(2)}) %all-to-all-start.2) | async-done | bytes 131104 | tf_op jit(solution)/shard_map/all_to_all | solution.py:54
  26.4 0.3 convolution_multiply_fusion.2
  26.7 0.4 multiply_reduce_fusion
  27.1 0.0 copy-start.2
  27.1 0.6 %copy-done.2 = f32[128]{0:T(128)S(1)} copy-done((f32[128]{0:T(128)S(1)}, f32[128]{0:T(128)}, u32[]{:S(2)}) %copy-start.2) | copy-done | bytes 536
  27.8 0.1 fusion.4
  27.8 0.2 copy.43
  28.0 0.5 %broadcast.100 = bf16[]{:T(256)} broadcast(bf16[]{:T(256)} %constant.141), dimensions={} | broadcast | bytes 4
  28.5 1.4 %reduce.2 = bf16[512,128]{1,0:T(8,128)(2,1)S(1)} reduce(bf16[512,1,1,128]{3,2,1,0:T(2,128)(2,1)S(1)} %bitcast.56, bf16[]{:T(256)} %broadcast.100), dimensions={1,2}, to_apply=%bitcast.43.reduce_sub_computation | reduce | bytes 262146
  30.0 7.0 %all_to_all.59 = bf16[4,2,8192]{2,1,0:T(2,128)(2,1)S(1)} all-to-all(bf16[4,2,8192]{2,1,0:T(2,128)(2,1)S(1)} %reshape.63), channel_id=1, replica_groups=mesh['sp'=4,'dp'=8] {'sp'}, dimensions={0} | all-to-all | bytes 262144 | tf_op jit(solution)/shard_map/all_to_all | solution.py:63
  37.0 0.1 reshape.64
  37.1 0.8 %copy.44 = bf16[1,128,4,128]{3,2,1,0:T(4,128)(2,1)} copy(bf16[1,128,4,128]{3,1,2,0:T(8,128)(2,1)S(1)} %bitcast.58) | data formatting | bytes 262144 | tf_op jit(solution)/shard_map/all_to_all | solution.py:63
  (6 shorter events, 0.1 us)
Async XLA Ops:
  1.6 4.4 %copy-start = (bf16[1,128,4,128]{3,2,1,0:T(4,128)(2,1)S(1)}, bf16[1,128,4,128]{3,2,1,0:T(4,128)(2,1)}, u32[]{:S(2)}) copy-start(bf16[1,128,4,128]{3,2,1,0:T(4,128)(2,1)} %param.7) | copy-start | bytes 393220
  1.6 9.0 %all-to-all-start = ((bf16[1,128,4,128]{3,1,0,2:T(8,128)(2,1)}), bf16[1,128,4,128]{3,1,0,2:T(8,128)(2,1)S(1)}, u32[]{:S(2)}, u32[]{:S(2)}) async-start(bf16[1,128,4,128]{3,1,0,2:T(8,128)(2,1)} %copy.33), calls=%async_computation | async-start | bytes 262144 | tf_op jit(solution)/shard_map/all_to_all | solution.py:51
  6.0 0.9 %copy-start.1 = (bf16[1,128,4,128]{3,2,1,0:T(4,128)(2,1)S(1)}, bf16[1,128,4,128]{3,2,1,0:T(4,128)(2,1)}, u32[]{:S(2)}) copy-start(bf16[1,128,4,128]{3,2,1,0:T(4,128)(2,1)} %param.6) | copy-start | bytes 393220
  10.6 7.9 %all-to-all-start.1 = ((bf16[1,128,4,128]{3,1,0,2:T(8,128)(2,1)}), bf16[1,128,4,128]{3,1,0,2:T(8,128)(2,1)S(1)}, u32[]{:S(2)}, u32[]{:S(2)}) async-start(bf16[1,128,4,128]{3,1,0,2:T(8,128)(2,1)} %copy.35), calls=%async_computation.1 | async-start | bytes 262144 | tf_op jit(solution)/shard_map/all_to_all | solution.py:52
  18.5 7.9 %all-to-all-start.2 = ((bf16[4,1,128,1,128]{4,2,3,1,0:T(8,128)(2,1)}), bf16[4,1,128,1,128]{4,2,3,1,0:T(8,128)(2,1)S(1)}, u32[]{:S(2)}, u32[]{:S(2)}) async-start(bf16[4,1,128,1,128]{4,2,3,1,0:T(8,128)(2,1)} %pad_maximum_fusion), calls=%async_computation.2 | async-start | bytes 262144 | tf_op jit(solution)/shard_map/all_to_all | solution.py:54
  27.1 0.7 %copy-start.2 = (f32[128]{0:T(128)S(1)}, f32[128]{0:T(128)}, u32[]{:S(2)}) copy-start(f32[128]{0:T(128)} %param.9) | copy-start | bytes 1540
